TPU v7x, 32 devices: a whole 2x2x4 slice. The times are simulated.
32 devices in a mesh: fs: 8 (over z, x), tp: 4 (over y, core).
Axes of the slice: x: 2, y: 2, z: 4, core: 2. Of those that a mesh axis runs over, the one named last changes fastest.
Arguments:
- tokens: bfloat16 [3072, 4096], P('fs', 'tp'), may hold values from -600 to 600
- gate_master: float32 [8, 4096, 512], P(None, 'fs', 'tp'), may hold values from -0.09375 to 0.09375
- up_master: float32 [8, 4096, 512], P(None, 'fs', 'tp'), may hold values from -0.09375 to 0.09375
- down_master: float32 [8, 4096, 512], P(None, 'fs', 'tp'), may hold values from -0.25 to 0.25
- norm_gain: float32 [4096], P('fs'), may hold values from 0.1 to 1.9
- routes: int32 [3072, 2], P('fs'), may hold values from 0 to 7, all different within a row; in each aligned block of 384 rows (0 to 383, 384 to 767, ...) at most 192 rows name the same one
- route_weight: float32 [3072, 2], P('fs'), may hold values from 0.1 to 1
Outputs:
- gate_out: bfloat16 [8, 4096, 512], P('fs', None, 'tp')
- up_out: bfloat16 [8, 4096, 512], P('fs', None, 'tp')
- down_out: bfloat16 [8, 4096, 512], P('fs', None, 'tp')
- mixed: bfloat16 [3072, 4096], P('fs', 'tp')
Inputs may be any that keep to these rules, and one draw needn't show every extreme that they name: `routes`: within the rows of one index of fs no expert is named by more than 192 pairs, a bound that some block reaches; the 2 experts of a row differ.
All inputs are finite; a program needn't handle non-finite values.
Results may differ from a plain program's by a relative error of at most 0.0087.
Values may be sent and summed in bfloat16 or wider, within the bound.
A program may use at most 128 MiB of HBM per device.

v0:
```python
import jax
import jax.numpy as jnp
from jax import lax
from jax.sharding import PartitionSpec as P

norm_eps = 1e-06


def slot_table(expert_ids, n_experts, capacity, top_count):
    assigned = expert_ids.shape[0]
    onehot = (expert_ids[:, None] == jnp.arange(n_experts, dtype=jnp.int32)[None, :]).astype(
        jnp.int32
    )
    before = jnp.cumsum(onehot, axis=0) - onehot
    slots = jnp.sum(before * onehot, axis=1)
    position = expert_ids * capacity + slots
    owners = jnp.arange(assigned, dtype=jnp.int32) // top_count
    matches = position[None, :] == jnp.arange(n_experts * capacity, dtype=jnp.int32)[:, None]
    slot_token = jnp.max(jnp.where(matches, owners[None, :], -1), axis=1)
    return (position, slot_token)


def place_rows(normed, slot_token):
    padded = jnp.concatenate([normed, jnp.zeros((1, normed.shape[1]), normed.dtype)], axis=0)
    chosen = jnp.where(slot_token < 0, normed.shape[0], slot_token)
    return padded[chosen]


def body(tokens, gate_master, up_master, down_master, norm_gain, routes, route_weight):
    n_experts = gate_master.shape[0]
    tok_rows = routes.shape[0]
    top_count = routes.shape[1]
    capacity = 2 * tok_rows * top_count // n_experts
    folded = norm_gain[None, :, None]
    gate_cast = (gate_master * folded).astype(jnp.bfloat16)
    up_cast = (up_master * folded).astype(jnp.bfloat16)
    down_cast = down_master.astype(jnp.bfloat16)
    gate_out, up_out, down_out = (
        lax.all_to_all(gate_cast, "fs", split_axis=0, concat_axis=1, tiled=True),
        lax.all_to_all(up_cast, "fs", split_axis=0, concat_axis=1, tiled=True),
        lax.all_to_all(down_cast, "fs", split_axis=0, concat_axis=1, tiled=True),
    )
    flat_routes = routes.reshape(-1)
    position, slot_token = slot_table(flat_routes, n_experts, capacity, top_count)
    mix_weights = route_weight / jnp.sum(route_weight, axis=1, keepdims=True)
    gate_mat = gate_out[0]
    up_mat = up_out[0]
    token_float = tokens.astype(jnp.float32)
    full_width = token_float.shape[1] * lax.axis_size("tp")
    sumsquares = lax.psum(jnp.sum(token_float * token_float, axis=1), "tp")
    inverse = lax.rsqrt(sumsquares / full_width + norm_eps)[:, None]
    normed = (token_float * inverse).astype(jnp.bfloat16)
    outgoing = place_rows(normed, slot_token).reshape(n_experts, capacity, normed.shape[1])
    arrived = lax.all_to_all(outgoing, "fs", split_axis=0, concat_axis=0, tiled=True).reshape(
        -1, normed.shape[1]
    )
    segment = lax.all_gather(arrived, "tp", axis=1, tiled=True)
    gate_val = jnp.dot(segment, gate_mat, preferred_element_type=jnp.float32)
    up_val = jnp.dot(segment, up_mat, preferred_element_type=jnp.float32)
    hidden = (jax.nn.silu(gate_val) * up_val).astype(jnp.bfloat16)
    hidden_whole = lax.all_gather(hidden, "tp", axis=1, tiled=True)
    down_quarter = lax.all_to_all(down_out[0], "tp", split_axis=0, concat_axis=1, tiled=True)
    result = lax.dot_general(
        hidden_whole, down_quarter, (((1,), (1,)), ((), ())), preferred_element_type=jnp.float32
    )
    summed = result.astype(jnp.bfloat16)
    returned = lax.all_to_all(
        summed.reshape(-1, capacity, summed.shape[1]), "fs", split_axis=0, concat_axis=0, tiled=True
    )
    flat_back = returned.reshape(-1, summed.shape[1])
    picked = flat_back[position].astype(jnp.float32).reshape(tok_rows, top_count, summed.shape[1])
    mixed = jnp.sum(mix_weights[:, :, None] * picked, axis=1).astype(jnp.bfloat16)
    return (gate_out, up_out, down_out, mixed)


def solution(mesh):
    placed = (
        P("fs", "tp"),
        P(None, "fs", "tp"),
        P(None, "fs", "tp"),
        P(None, "fs", "tp"),
        P("fs"),
        P("fs", None),
        P("fs", None),
    )
    return jax.shard_map(
        body,
        mesh=mesh,
        in_specs=placed,
        out_specs=(P("fs", None, "tp"), P("fs", None, "tp"), P("fs", None, "tp"), P("fs", "tp")),
        check_vma=False,
    )
```

profile of v0, /device:TPU:0, one launch (start us, length us, event | category | flops | bytes accessed | tf_op | source)
XLA Modules:
  0.0 341.4 jit_solution(13418795608480970905)
XLA Ops:
  7.2 0.0 all-gather.3.cloned.1.call-start
  7.2 0.8 copy.28
  8.0 0.1 eq.39
  8.2 0.1 reshape.132
  8.3 1.7 reduce-window.6
  10.1 0.1 slice.12
  10.1 0.1 copy.30
  10.3 0.2 reduce-window.9
  10.4 0.1 copy.31
  10.5 0.1 fusion.4
  10.6 0.7 select_reduce_fusion
  11.4 1.4 fusion.1
  12.7 8.4 %psum.7 = f32[384]{0:T(512)S(1)} all-reduce(f32[384]{0:T(512)S(1)} %fusion.1), channel_id=1, replica_groups=mesh['fs'=8,'tp'=4] {'tp'}, use_global_device_ids=true, to_apply=%region_2.3 | all-reduce | flops 384 | bytes 3072 | tf_op jit(solution)/shard_map/psum | solution.py:50
  21.1 1.3 fusion.2
  22.5 0.1 concatenate.3
  22.5 5.8 %gather_fusion = bf16[1536,1024]{1,0:T(8,128)(2,1)} fusion(bf16[385,1024]{1,0:T(8,128)(2,1)S(1)} %concatenate.3, s32[2048]{0:T(1024)S(1)} %pad_clamp_fusion), kind=kCustom, calls=%fused_computation | custom fusion | bytes 6297600 | tf_op jit(solution)/shard_map/gather | solution.py:26
  28.4 75.4 %all_to_all.65 = bf16[8,192,1024]{2,1,0:T(8,128)(2,1)} all-to-all(bf16[8,192,1024]{2,1,0:T(8,128)(2,1)} %bitcast.30), channel_id=1, replica_groups=mesh['fs'=8,'tp'=4] {'fs'}, dimensions={0} | all-to-all | bytes 6291456 | tf_op jit(solution)/shard_map/all_to_all | solution.py:54
  103.8 0.0 all-gather.3.cloned.1.call-update
  103.8 1.6 copy-done.6
  105.4 3.0 multiply_convert_fusion
  108.3 28.8 %all_to_all.66 = bf16[8,512,128]{2,1,0:T(8,128)(2,1)S(1)} all-to-all(bf16[8,512,128]{2,1,0:T(8,128)(2,1)S(1)} %get-tuple-element.5), channel_id=1, replica_groups=mesh['fs'=8,'tp'=4] {'fs'}, dimensions={0} | all-to-all | bytes 2097152 | tf_op jit(solution)/shard_map/all_to_all | solution.py:39
  137.1 3.6 %all-to-all-start.1 = ((bf16[8,512,128]{2,1,0:T(8,128)(2,1)}), bf16[8,512,128]{2,1,0:T(8,128)(2,1)S(1)}, u32[]{:S(2)}, u32[]{:S(2)}) async-start(bf16[8,512,128]{2,1,0:T(8,128)(2,1)} %get-tuple-element.4), calls=%async_computation.1 | async-start | bytes 2097152 | tf_op jit(solution)/shard_map/all_to_all | solution.py:40
  140.7 2.7 convert_element_type.40
  143.4 41.7 %all-gather.3.cloned.1.call-done = bf16[1536,4096]{1,0:T(8,128)(2,1)} async-done(((bf16[1536,1024]{1,0:T(8,128)(2,1)}), bf16[1536,4096]{1,0:T(8,128)(2,1)}) %all-gather.3.cloned.1.call-update) | async-done | bytes 12582928 | tf_op jit(solution)/shard_map/all_gather | solution.py:57
  185.1 6.4 %fusion.11 = f32[1536,128]{1,0:T(8,128)S(1)} fusion(bf16[1536,4096]{1,0:T(8,128)(2,1)} %all-gather.3.cloned.1.call-done, bf16[4096,128]{1,0:T(8,128)(2,1)S(1)} %bitcast.33), kind=kOutput, calls=%fused_computation.38 | convolution fusion | flops 1610612736 | bytes 14417920 | tf_op jit(solution)/shard_map/dot_general | solution.py:58
  191.5 0.0 copy-start.4
  191.5 5.5 %all-to-all-start.2 = ((bf16[8,512,128]{2,1,0:T(8,128)(2,1)}), bf16[8,512,128]{2,1,0:T(8,128)(2,1)S(1)}, u32[]{:S(2)}, u32[]{:S(2)}) async-start(bf16[8,512,128]{2,1,0:T(8,128)(2,1)} %convert_element_type.40), calls=%async_computation.2 | async-start | bytes 2097152 | tf_op jit(solution)/shard_map/all_to_all | solution.py:41
  197.1 0.0 all-gather.5.cloned.1.call-start
  197.1 7.4 %fusion = bf16[1536,128]{1,0:T(8,128)(2,1)} fusion(bf16[1536,4096]{1,0:T(8,128)(2,1)} %all-gather.3.cloned.1.call-done, bf16[4096,128]{1,0:T(8,128)(2,1)S(1)} %bitcast.35, f32[1536,128]{1,0:T(8,128)S(1)} %fusion.11), kind=kOutput, calls=%fused_computation.7 | convolution fusion | flops 1611792384 | bytes 14811136 | tf_op jit(solution)/shard_map/dot_general | solution.py:59
  204.5 0.0 all-gather.5.cloned.1.call-update
  204.5 18.7 %all-to-all-done.2 = bf16[8,512,128]{2,1,0:T(8,128)(2,1)S(1)} async-done(((bf16[8,512,128]{2,1,0:T(8,128)(2,1)}), bf16[8,512,128]{2,1,0:T(8,128)(2,1)S(1)}, u32[]{:S(2)}, u32[]{:S(2)}) %all-to-all-start.2) | async-done | bytes 1048608 | tf_op jit(solution)/shard_map/all_to_all | solution.py:41
  223.3 16.8 %all_to_all.67 = bf16[4,1024,128]{2,1,0:T(8,128)(2,1)S(1)} all-to-all(bf16[4,1024,128]{2,1,0:T(8,128)(2,1)S(1)} %bitcast.31), channel_id=1, replica_groups=mesh['fs'=8,'tp'=4] {'tp'}, dimensions={0} | all-to-all | bytes 2097152 | tf_op jit(solution)/shard_map/all_to_all | solution.py:62
  240.1 0.5 copy.32
  240.6 0.0 all-gather.5.cloned.1.call-done
  240.7 4.9 %convolution_convert_fusion = bf16[1536,1024]{1,0:T(8,128)(2,1)} fusion(bf16[1536,512]{1,0:T(8,128)(2,1)} %all-gather.5.cloned.1.call-done, bf16[1024,512]{0,1:T(8,128)(2,1)S(1)} %bitcast.39), kind=kOutput, calls=%fused_computation.4 | convolution fusion | flops 1612185600 | bytes 5767168 | tf_op jit(solution)/shard_map/dot_general | solution.py:63
  245.5 4.0 %all-to-all-start.5 = ((bf16[8,192,1024]{2,1,0:T(8,128)(2,1)}), bf16[8,192,1024]{2,1,0:T(8,128)(2,1)S(1)}, u32[]{:S(2)}, u32[]{:S(2)}) async-start(bf16[8,192,1024]{2,1,0:T(8,128)(2,1)} %bitcast.38), calls=%async_computation.5 | async-start | bytes 6291456 | tf_op jit(solution)/shard_map/all_to_all | solution.py:67
  249.5 0.1 copy.33
  249.7 0.2 mul.81
  249.9 0.1 copy.27
  250.1 69.8 %all-to-all-done.5 = bf16[8,192,1024]{2,1,0:T(8,128)(2,1)S(1)} async-done(((bf16[8,192,1024]{2,1,0:T(8,128)(2,1)}), bf16[8,192,1024]{2,1,0:T(8,128)(2,1)S(1)}, u32[]{:S(2)}, u32[]{:S(2)}) %all-to-all-start.5) | async-done | bytes 3145760 | tf_op jit(solution)/shard_map/all_to_all | solution.py:67
  319.9 3.6 %gather_fusion.1 = bf16[768,1024]{1,0:T(8,128)(2,1)} fusion(bf16[1536,1024]{1,0:T(8,128)(2,1)S(1)} %bitcast.28, s32[1024]{0:T(1024)S(1)} %pad_clamp_fusion.1), kind=kCustom, calls=%fused_computation.1 | custom fusion | bytes 3148800 | tf_op jit(solution)/shard_map/gather | solution.py:71
  323.4 3.4 reshape.138
  326.8 0.0 copy-start.3
  326.9 0.0 copy-start.5
  326.9 4.8 %multiply_reduce_fusion = bf16[384,1024]{1,0:T(8,128)(2,1)} fusion(f32[384,2,1024]{2,1,0:T(2,128)S(1)} %reshape.138, f32[384,2]{1,0:T(8,128)S(1)} %copy.27), kind=kLoop, calls=%fused_computation.5 | loop fusion | flops 1179648 | bytes 3935232 | tf_op jit(solution)/shard_map/reduce_sum | solution.py:72
  331.7 1.0 copy.37
  332.7 1.0 copy.38
  333.6 1.0 copy.39
  (27 shorter events, 0.1 us)
Async XLA Ops:
  7.2 177.9 %all-gather.3.cloned.1.call-start = ((), (), s32[]{:S(2)}) async-start(), calls=%async_computation.6 | async-start | bytes 15728640 | tf_op jit(solution)/shard_map/all_gather | solution.py:57
  103.8 1.6 copy-start.6
  103.8 1.6 copy-start.9
  137.1 54.4 %copy-start.2 = (bf16[8,512,128]{2,1,0:T(8,128)(2,1)}, bf16[8,512,128]{2,1,0:T(8,128)(2,1)S(1)}, u32[]{:S(2)}) copy-start(bf16[8,512,128]{2,1,0:T(8,128)(2,1)S(1)} %all_to_all.66) | copy-start | bytes 3145732
  137.1 54.4 %all-to-all-start.1 = ((bf16[8,512,128]{2,1,0:T(8,128)(2,1)}), bf16[8,512,128]{2,1,0:T(8,128)(2,1)S(1)}, u32[]{:S(2)}, u32[]{:S(2)}) async-start(bf16[8,512,128]{2,1,0:T(8,128)(2,1)} %get-tuple-element.4), calls=%async_computation.1 | async-start | bytes 2097152 | tf_op jit(solution)/shard_map/all_to_all | solution.py:40
  191.5 13.0 %copy-start.4 = (bf16[8,512,128]{2,1,0:T(8,128)(2,1)}, bf16[8,512,128]{2,1,0:T(8,128)(2,1)S(1)}, u32[]{:S(2)}) copy-start(bf16[8,512,128]{2,1,0:T(8,128)(2,1)S(1)} %all-to-all-done.1) | copy-start | bytes 3145732
  191.5 31.7 %all-to-all-start.2 = ((bf16[8,512,128]{2,1,0:T(8,128)(2,1)}), bf16[8,512,128]{2,1,0:T(8,128)(2,1)S(1)}, u32[]{:S(2)}, u32[]{:S(2)}) async-start(bf16[8,512,128]{2,1,0:T(8,128)(2,1)} %convert_element_type.40), calls=%async_computation.2 | async-start | bytes 2097152 | tf_op jit(solution)/shard_map/all_to_all | solution.py:41
  197.1 43.6 %all-gather.5.cloned.1.call-start = ((), (), s32[]{:S(2)}) async-start(), calls=%async_computation.7 | async-start | bytes 1966080 | tf_op jit(solution)/shard_map/all_gather | solution.py:61
  223.3 22.3 %copy-start = (bf16[8,512,128]{2,1,0:T(8,128)(2,1)}, bf16[8,512,128]{2,1,0:T(8,128)(2,1)S(1)}, u32[]{:S(2)}) copy-start(bf16[8,512,128]{2,1,0:T(8,128)(2,1)S(1)} %all-to-all-done.2) | copy-start | bytes 3145732
  245.5 4.0 %copy-start.8 = (s32[384,2]{0,1:T(2,128)S(1)}, s32[384,2]{0,1:T(2,128)}, u32[]{:S(2)}) copy-start(s32[384,2]{0,1:T(2,128)} %param.12) | copy-start | bytes 9220
  245.5 4.3 %copy-start.7 = (f32[384,2]{0,1:T(2,128)S(1)}, f32[384,2]{0,1:T(2,128)}, u32[]{:S(2)}) copy-start(f32[384,2]{0,1:T(2,128)} %param.13) | copy-start | bytes 9220
  245.5 74.3 %all-to-all-start.5 = ((bf16[8,192,1024]{2,1,0:T(8,128)(2,1)}), bf16[8,192,1024]{2,1,0:T(8,128)(2,1)S(1)}, u32[]{:S(2)}, u32[]{:S(2)}) async-start(bf16[8,192,1024]{2,1,0:T(8,128)(2,1)} %bitcast.38), calls=%async_computation.5 | async-start | bytes 6291456 | tf_op jit(solution)/shard_map/all_to_all | solution.py:67
  326.8 4.8 %copy-start.3 = (bf16[8,512,128]{2,1,0:T(8,128)(2,1)S(1)}, bf16[8,512,128]{2,1,0:T(8,128)(2,1)}, u32[]{:S(2)}) copy-start(bf16[8,512,128]{2,1,0:T(8,128)(2,1)} %copy-done.2) | copy-start | bytes 3145732
  326.9 5.8 %copy-start.5 = (bf16[8,512,128]{2,1,0:T(8,128)(2,1)S(1)}, bf16[8,512,128]{2,1,0:T(8,128)(2,1)}, u32[]{:S(2)}) copy-start(bf16[8,512,128]{2,1,0:T(8,128)(2,1)} %copy-done.4) | copy-start | bytes 3145732
  326.9 6.8 %copy-start.1 = (bf16[8,512,128]{2,1,0:T(8,128)(2,1)S(1)}, bf16[8,512,128]{2,1,0:T(8,128)(2,1)}, u32[]{:S(2)}) copy-start(bf16[8,512,128]{2,1,0:T(8,128)(2,1)} %copy-done) | copy-start | bytes 3145732
Sparse Core Ops, SparseCore 0:
  103.9 81.1 all-gather.2
  204.6 20.2 all-gather.4
where the time goes:
time: 342 us; the launch traced here: 341 us
  waiting for transfers between devices  130 us (38%)
  blocking collectives  129 us (38%)
  local copies, waits for them, and re-layouts  19.7 us (6%)
  matrix products  18.6 us (5%)
  other arithmetic  16 us (5%)
  between operations  14.3 us (4%)
  starting transfers between devices  13.1 us (4%)
    all_to_all x1, blocking collectives, body(): lax.all_to_all(outgoing, 'fs', split_axis=0, concat_axis=0, tiled=True)  75.4 us
    all_to_all x1, waiting for transfers between devices, body(): lax.all_to_all(summed.reshape(-1, capacity, summed.shape[1]), 'fs', split...  69.8 us
    all_gather x1, waiting for transfers between devices, body(): segment = lax.all_gather(arrived, 'tp', axis=1, tiled=True)  41.7 us
    all_to_all x1, blocking collectives, body(): lax.all_to_all(gate_cast, 'fs', split_axis=0, concat_axis=1, tiled=True)  28.8 us
    all_to_all x1, waiting for transfers between devices, body(): lax.all_to_all(down_cast, 'fs', split_axis=0, concat_axis=1, tiled=True)  18.7 us
    all_to_all x1, blocking collectives, body(): lax.all_to_all(down_out[0], 'tp', split_axis=0, concat_axis=1, tiled=True)  16.8 us
    psum x1, blocking collectives, body(): sumsquares = lax.psum(jnp.sum(token_float * token_float, axis=1), 'tp')  8.39 us
    dot_general x1, matrix products, body(): up_val = jnp.dot(segment, up_mat, preferred_element_type=jnp.float32)  7.37 us
  transfers between devices with their start and end apart: 5, of which 3 were waited for; matrix products, arithmetic and copies ran while one was open for 6% of the time, Pallas kernels for 0%

commit v1 on v0

--- a/solution.py
+++ b/solution.py
@@ -38,7 +38,12 @@
     gate_out, up_out, down_out = (
         lax.all_to_all(gate_cast, "fs", split_axis=0, concat_axis=1, tiled=True),
         lax.all_to_all(up_cast, "fs", split_axis=0, concat_axis=1, tiled=True),
-        lax.all_to_all(down_cast, "fs", split_axis=0, concat_axis=1, tiled=True),
+        jnp.concatenate(
+            lax.all_to_all(
+                jnp.stack(jnp.split(down_cast, lax.axis_size("fs"), axis=0)), "fs", 0, 0
+            ),
+            axis=1,
+        ),
     )
     flat_routes = routes.reshape(-1)
     position, slot_token = slot_table(flat_routes, n_experts, capacity, top_count)

time: 342 us -> 342 us (level)
  blocking collectives: 129 us -> 101 us
  waiting for transfers between devices: 130 us -> 150 us
  local copies, waits for them, and re-layouts: 19.7 us -> 25.1 us
  starting transfers between devices: 13.1 us -> 16.7 us
    all_to_all x1 -> x0, blocking collectives: 28.8 us -> none  [body(): lax.all_to_all(gate_cast, 'fs', split_axis=0, concat_axis=1, tiled=True)]
    all_to_all x1 -> x2, waiting for transfers between devices: 18.7 us -> 38.7 us  [the longest x1 20 us: body(): lax.all_to_all(gate_cast, 'fs', split_axis=0, concat_axis=1, tiled=True)]
    unnamed x24 -> x31, local copies, waits for them, and re-layouts: 5.33 us -> 9.98 us
    all_to_all x1 -> x2, starting transfers between devices: 5.53 us -> 9.11 us  [the longest x1 5.52 us: body(): lax.all_to_all(jnp.stack(jnp.split(down_cast, lax.axis_size('fs'), axis=0...]
  transfers between devices with their start and end apart: 5 -> 6, of which waited for: 3 -> 4; matrix products, arithmetic and copies ran while one was open for 6% -> 8% of each run, Pallas kernels for 0% -> 0%
where the time goes in v1:
time: 342 us; the launch traced here: 341 us
  waiting for transfers between devices  150 us (44%)
  blocking collectives  101 us (30%)
  local copies, waits for them, and re-layouts  25.1 us (7%)
  matrix products  18.6 us (5%)
  starting transfers between devices  16.7 us (5%)
  other arithmetic  15.9 us (5%)
  between operations  14.3 us (4%)
    all_to_all x1, blocking collectives, body(): lax.all_to_all(outgoing, 'fs', split_axis=0, concat_axis=0, tiled=True)  75.4 us
    all_to_all x1, waiting for transfers between devices, body(): lax.all_to_all(summed.reshape(-1, capacity, summed.shape[1]), 'fs', split...  69.8 us
    all_gather x1, waiting for transfers between devices, body(): segment = lax.all_gather(arrived, 'tp', axis=1, tiled=True)  41.6 us
    all_to_all x1, waiting for transfers between devices, body(): lax.all_to_all(gate_cast, 'fs', split_axis=0, concat_axis=1, tiled=True)  20 us
    all_to_all x1, waiting for transfers between devices, body(): lax.all_to_all(jnp.stack(jnp.split(down_cast, lax.axis_size('fs'), axis=0...  18.7 us
    all_to_all x1, blocking collectives, body(): lax.all_to_all(down_out[0], 'tp', split_axis=0, concat_axis=1, tiled=True)  16.8 us
    unnamed x31, local copies, waits for them, and re-layouts  9.98 us
    psum x1, blocking collectives, body(): sumsquares = lax.psum(jnp.sum(token_float * token_float, axis=1), 'tp')  8.39 us
  transfers between devices with their start and end apart: 6, of which 4 were waited for; matrix products, arithmetic and copies ran while one was open for 8% of the time, Pallas kernels for 0%

profile of v1, /device:TPU:0, one launch (start us, length us, event | category | flops | bytes accessed | tf_op | source)
XLA Modules:
  0.0 341.4 jit_solution(10141146430103839362)
XLA Ops:
  7.2 0.8 copy.42
  8.0 0.1 eq.39
  8.2 0.1 reshape.132
  8.3 1.7 reduce-window.6
  10.1 0.1 slice.12
  10.1 0.1 copy.44
  10.3 0.2 reduce-window.9
  10.4 0.1 copy.45
  10.5 0.1 fusion.12
  10.6 0.7 select_reduce_fusion
  11.4 1.4 fusion.1
  12.7 8.4 %psum.7 = f32[384]{0:T(512)S(1)} all-reduce(f32[384]{0:T(512)S(1)} %fusion.1), channel_id=1, replica_groups=mesh['fs'=8,'tp'=4] {'tp'}, use_global_device_ids=true, to_apply=%region_2.3 | all-reduce | flops 384 | bytes 3072 | tf_op jit(solution)/shard_map/psum | solution.py:55
  21.1 1.3 fusion.2
  22.5 5.8 %gather_fusion = bf16[1536,1024]{1,0:T(8,128)(2,1)} fusion(bf16[385,1024]{1,0:T(8,128)(2,1)S(1)} %concatenate.3, s32[2048]{0:T(1024)S(1)} %pad_clamp_fusion), kind=kCustom, calls=%fused_computation | custom fusion | bytes 6297600 | tf_op jit(solution)/shard_map/gather | solution.py:26
  28.4 75.4 %all_to_all.58 = bf16[8,192,1024]{2,1,0:T(8,128)(2,1)} all-to-all(bf16[8,192,1024]{2,1,0:T(8,128)(2,1)} %bitcast.62), channel_id=1, replica_groups=mesh['fs'=8,'tp'=4] {'fs'}, dimensions={0} | all-to-all | bytes 6291456 | tf_op jit(solution)/shard_map/all_to_all | solution.py:59
  103.8 1.6 copy-done.6
  105.4 3.5 %multiply_convert_fusion = (bf16[8,512,128]{2,1,0:T(8,128)(2,1)}, bf16[8,512,128]{2,1,0:T(8,128)(2,1)}) fusion(f32[8,512,128]{2,1,0:T(8,128)S(1)} %copy-done.6, f32[512]{0:T(512)S(1)} %copy-done.9, f32[8,512,128]{2,1,0:T(8,128)} %param.8), kind=kLoop, calls=%fused_computation.8 | loop fusion | flops 2097152 | bytes 6293504 | tf_op jit(solution)/shard_map/convert_element_type | solution.py:36
  108.8 3.6 %all-to-all-start = ((bf16[8,512,128]{2,1,0:T(8,128)(2,1)}), bf16[8,512,128]{2,1,0:T(8,128)(2,1)S(1)}, u32[]{:S(2)}, u32[]{:S(2)}) async-start(bf16[8,512,128]{2,1,0:T(8,128)(2,1)} %get-tuple-element.5), calls=%async_computation | async-start | bytes 2097152 | tf_op jit(solution)/shard_map/all_to_all | solution.py:39
  112.4 2.2 convert_element_type.40
  114.6 0.7 fusion.10
  115.3 0.7 fusion.9
  116.0 0.7 fusion.8
  116.6 0.7 fusion.7
  117.3 0.7 fusion.6
  117.9 20.0 %all-to-all-done = bf16[8,512,128]{2,1,0:T(8,128)(2,1)S(1)} async-done(((bf16[8,512,128]{2,1,0:T(8,128)(2,1)}), bf16[8,512,128]{2,1,0:T(8,128)(2,1)S(1)}, u32[]{:S(2)}, u32[]{:S(2)}) %all-to-all-start) | async-done | bytes 1048608 | tf_op jit(solution)/shard_map/all_to_all | solution.py:39
  137.9 3.6 %all-to-all-start.1 = ((bf16[8,512,128]{2,1,0:T(8,128)(2,1)}), bf16[8,512,128]{2,1,0:T(8,128)(2,1)S(1)}, u32[]{:S(2)}, u32[]{:S(2)}) async-start(bf16[8,512,128]{2,1,0:T(8,128)(2,1)} %get-tuple-element.4), calls=%async_computation.1 | async-start | bytes 2097152 | tf_op jit(solution)/shard_map/all_to_all | solution.py:40
  141.5 0.7 fusion.5
  142.2 0.7 fusion.4
  142.8 0.7 fusion.3
  143.5 41.6 %all-gather.3.cloned.1.call-done = bf16[1536,4096]{1,0:T(8,128)(2,1)} async-done(((bf16[1536,1024]{1,0:T(8,128)(2,1)}), bf16[1536,4096]{1,0:T(8,128)(2,1)}) %all-gather.3.cloned.1.call-update) | async-done | bytes 12582928 | tf_op jit(solution)/shard_map/all_gather | solution.py:62
  185.1 6.4 %fusion.19 = f32[1536,128]{1,0:T(8,128)S(1)} fusion(bf16[1536,4096]{1,0:T(8,128)(2,1)} %all-gather.3.cloned.1.call-done, bf16[4096,128]{1,0:T(8,128)(2,1)S(1)} %bitcast.65), kind=kOutput, calls=%fused_computation.54 | convolution fusion | flops 1610612736 | bytes 14417920 | tf_op jit(solution)/shard_map/dot_general | solution.py:63
  191.5 5.5 %all-to-all-start.2 = ((bf16[8,1,512,128]{3,2,1,0:T(8,128)(2,1)}), bf16[8,1,512,128]{3,2,1,0:T(8,128)(2,1)S(1)}, u32[]{:S(2)}, u32[]{:S(2)}) async-start(bf16[8,1,512,128]{3,2,1,0:T(8,128)(2,1)} %fusion.3), calls=%async_computation.2 | async-start | bytes 2097152 | tf_op jit(solution)/shard_map/all_to_all | solution.py:42
  197.1 7.4 %fusion = bf16[1536,128]{1,0:T(8,128)(2,1)} fusion(bf16[1536,4096]{1,0:T(8,128)(2,1)} %all-gather.3.cloned.1.call-done, bf16[4096,128]{1,0:T(8,128)(2,1)S(1)} %bitcast.67, f32[1536,128]{1,0:T(8,128)S(1)} %fusion.19), kind=kOutput, calls=%fused_computation.7 | convolution fusion | flops 1611792384 | bytes 14811136 | tf_op jit(solution)/shard_map/dot_general | solution.py:64
  204.5 18.7 %all-to-all-done.2 = bf16[8,1,512,128]{3,2,1,0:T(8,128)(2,1)S(1)} async-done(((bf16[8,1,512,128]{3,2,1,0:T(8,128)(2,1)}), bf16[8,1,512,128]{3,2,1,0:T(8,128)(2,1)S(1)}, u32[]{:S(2)}, u32[]{:S(2)}) %all-to-all-start.2) | async-done | bytes 1048608 | tf_op jit(solution)/shard_map/all_to_all | solution.py:42
  223.3 16.8 %all_to_all.59 = bf16[4,1024,128]{2,1,0:T(8,128)(2,1)S(1)} all-to-all(bf16[4,1024,128]{2,1,0:T(8,128)(2,1)S(1)} %bitcast.63), channel_id=1, replica_groups=mesh['fs'=8,'tp'=4] {'tp'}, dimensions={0} | all-to-all | bytes 2097152 | tf_op jit(solution)/shard_map/all_to_all | solution.py:67
  240.1 0.5 copy.46
  240.7 4.9 %convolution_convert_fusion = bf16[1536,1024]{1,0:T(8,128)(2,1)} fusion(bf16[1536,512]{1,0:T(8,128)(2,1)} %all-gather.5.cloned.1.call-done, bf16[1024,512]{0,1:T(8,128)(2,1)S(1)} %bitcast.71), kind=kOutput, calls=%fused_computation.4 | convolution fusion | flops 1612185600 | bytes 5767168 | tf_op jit(solution)/shard_map/dot_general | solution.py:68
  245.5 4.0 %all-to-all-start.5 = ((bf16[8,192,1024]{2,1,0:T(8,128)(2,1)}), bf16[8,192,1024]{2,1,0:T(8,128)(2,1)S(1)}, u32[]{:S(2)}, u32[]{:S(2)}) async-start(bf16[8,192,1024]{2,1,0:T(8,128)(2,1)} %bitcast.70), calls=%async_computation.5 | async-start | bytes 6291456 | tf_op jit(solution)/shard_map/all_to_all | solution.py:72
  249.5 0.1 copy.47
  249.7 0.2 mul.81
  249.9 0.1 copy.41
  250.1 69.8 %all-to-all-done.5 = bf16[8,192,1024]{2,1,0:T(8,128)(2,1)S(1)} async-done(((bf16[8,192,1024]{2,1,0:T(8,128)(2,1)}), bf16[8,192,1024]{2,1,0:T(8,128)(2,1)S(1)}, u32[]{:S(2)}, u32[]{:S(2)}) %all-to-all-start.5) | async-done | bytes 3145760 | tf_op jit(solution)/shard_map/all_to_all | solution.py:72
  319.9 3.6 %gather_fusion.1 = bf16[768,1024]{1,0:T(8,128)(2,1)} fusion(bf16[1536,1024]{1,0:T(8,128)(2,1)S(1)} %bitcast.60, s32[1024]{0:T(1024)S(1)} %pad_clamp_fusion.1), kind=kCustom, calls=%fused_computation.1 | custom fusion | bytes 3148800 | tf_op jit(solution)/shard_map/gather | solution.py:76
  323.4 3.4 reshape.138
  326.9 4.8 %multiply_reduce_fusion = bf16[384,1024]{1,0:T(8,128)(2,1)} fusion(f32[384,2,1024]{2,1,0:T(2,128)S(1)} %reshape.138, f32[384,2]{1,0:T(8,128)S(1)} %copy.41), kind=kLoop, calls=%fused_computation.5 | loop fusion | flops 1179648 | bytes 3935232 | tf_op jit(solution)/shard_map/reduce_sum | solution.py:77
  331.7 1.0 copy.58
  332.7 1.0 copy.59
  333.6 1.0 copy.60
  (36 shorter events, 0.3 us)
Async XLA Ops:
  7.2 177.9 %all-gather.3.cloned.1.call-start = ((), (), s32[]{:S(2)}) async-start(), calls=%async_computation.6 | async-start | bytes 15728640 | tf_op jit(solution)/shard_map/all_gather | solution.py:62
  103.8 1.6 copy-start.6
  103.8 1.6 copy-start.9
  108.8 29.1 %all-to-all-start = ((bf16[8,512,128]{2,1,0:T(8,128)(2,1)}), bf16[8,512,128]{2,1,0:T(8,128)(2,1)S(1)}, u32[]{:S(2)}, u32[]{:S(2)}) async-start(bf16[8,512,128]{2,1,0:T(8,128)(2,1)} %get-tuple-element.5), calls=%async_computation | async-start | bytes 2097152 | tf_op jit(solution)/shard_map/all_to_all | solution.py:39
  137.9 53.6 %copy-start.2 = (bf16[8,512,128]{2,1,0:T(8,128)(2,1)}, bf16[8,512,128]{2,1,0:T(8,128)(2,1)S(1)}, u32[]{:S(2)}) copy-start(bf16[8,512,128]{2,1,0:T(8,128)(2,1)S(1)} %all-to-all-done) | copy-start | bytes 3145732
  137.9 53.6 %all-to-all-start.1 = ((bf16[8,512,128]{2,1,0:T(8,128)(2,1)}), bf16[8,512,128]{2,1,0:T(8,128)(2,1)S(1)}, u32[]{:S(2)}, u32[]{:S(2)}) async-start(bf16[8,512,128]{2,1,0:T(8,128)(2,1)} %get-tuple-element.4), calls=%async_computation.1 | async-start | bytes 2097152 | tf_op jit(solution)/shard_map/all_to_all | solution.py:40
  191.5 12.9 %copy-start.4 = (bf16[8,512,128]{2,1,0:T(8,128)(2,1)}, bf16[8,512,128]{2,1,0:T(8,128)(2,1)S(1)}, u32[]{:S(2)}) copy-start(bf16[8,512,128]{2,1,0:T(8,128)(2,1)S(1)} %all-to-all-done.1) | copy-start | bytes 3145732
  191.5 31.7 %all-to-all-start.2 = ((bf16[8,1,512,128]{3,2,1,0:T(8,128)(2,1)}), bf16[8,1,512,128]{3,2,1,0:T(8,128)(2,1)S(1)}, u32[]{:S(2)}, u32[]{:S(2)}) async-start(bf16[8,1,512,128]{3,2,1,0:T(8,128)(2,1)} %fusion.3), calls=%async_computation.2 | async-start | bytes 2097152 | tf_op jit(solution)/shard_map/all_to_all | solution.py:42
  197.1 43.6 %all-gather.5.cloned.1.call-start = ((), (), s32[]{:S(2)}) async-start(), calls=%async_computation.7 | async-start | bytes 1966080 | tf_op jit(solution)/shard_map/all_gather | solution.py:66
  223.3 22.3 %copy-start = (bf16[8,1,512,128]{3,2,1,0:T(8,128)(2,1)}, bf16[8,1,512,128]{3,2,1,0:T(8,128)(2,1)S(1)}, u32[]{:S(2)}) copy-start(bf16[8,1,512,128]{3,2,1,0:T(8,128)(2,1)S(1)} %all-to-all-done.2) | copy-start | bytes 3145732
  245.5 4.0 %copy-start.8 = (s32[384,2]{0,1:T(2,128)S(1)}, s32[384,2]{0,1:T(2,128)}, u32[]{:S(2)}) copy-start(s32[384,2]{0,1:T(2,128)} %param.12) | copy-start | bytes 9220
  245.5 4.3 %copy-start.7 = (f32[384,2]{0,1:T(2,128)S(1)}, f32[384,2]{0,1:T(2,128)}, u32[]{:S(2)}) copy-start(f32[384,2]{0,1:T(2,128)} %param.13) | copy-start | bytes 9220
  245.5 74.3 %all-to-all-start.5 = ((bf16[8,192,1024]{2,1,0:T(8,128)(2,1)}), bf16[8,192,1024]{2,1,0:T(8,128)(2,1)S(1)}, u32[]{:S(2)}, u32[]{:S(2)}) async-start(bf16[8,192,1024]{2,1,0:T(8,128)(2,1)} %bitcast.70), calls=%async_computation.5 | async-start | bytes 6291456 | tf_op jit(solution)/shard_map/all_to_all | solution.py:72
  326.8 4.8 %copy-start.3 = (bf16[8,512,128]{2,1,0:T(8,128)(2,1)S(1)}, bf16[8,512,128]{2,1,0:T(8,128)(2,1)}, u32[]{:S(2)}) copy-start(bf16[8,512,128]{2,1,0:T(8,128)(2,1)} %copy-done.2) | copy-start | bytes 3145732
  326.9 5.8 %copy-start.5 = (bf16[8,512,128]{2,1,0:T(8,128)(2,1)S(1)}, bf16[8,512,128]{2,1,0:T(8,128)(2,1)}, u32[]{:S(2)}) copy-start(bf16[8,512,128]{2,1,0:T(8,128)(2,1)} %copy-done.4) | copy-start | bytes 3145732
  326.9 6.8 %copy-start.1 = (bf16[8,1,512,128]{3,2,1,0:T(8,128)(2,1)S(1)}, bf16[8,1,512,128]{3,2,1,0:T(8,128)(2,1)}, u32[]{:S(2)}) copy-start(bf16[8,1,512,128]{3,2,1,0:T(8,128)(2,1)} %copy-done) | copy-start | bytes 3145732
Sparse Core Ops, SparseCore 0:
  103.9 81.1 all-gather.2
  204.6 20.2 all-gather.4
